TPU v7x, 32 devices: a whole 2x2x4 slice. The times are simulated.
32 devices in a mesh: sp: 8 (over z, core), tp: 4 (over y, x).
Axes of the slice: x: 2, y: 2, z: 4, core: 2. Of those that a mesh axis runs over, the one named last changes fastest.
Arguments:
- stream: bfloat16 [1024, 2048], P('sp'), may hold values from -6 to 6
- query_small: bfloat16 [1024, 1024], P('sp', 'tp'), may hold values from -6 to 6
- key_small: bfloat16 [1024, 1024], P('sp', 'tp'), may hold values from -6 to 6
- value_small: bfloat16 [1024, 1024], P('sp', 'tp'), may hold values from -6 to 6
- query_large: bfloat16 [1024, 2048], P('sp', 'tp'), may hold values from -6 to 6
- key_large: bfloat16 [1024, 2048], P('sp', 'tp'), may hold values from -6 to 6
- value_large: bfloat16 [1024, 2048], P('sp', 'tp'), may hold values from -6 to 6
- key_bias: bfloat16 [1024, 2, 16], P('sp', None, 'tp'), may hold values from -16 to 1
- out_small: bfloat16 [1024, 2048], P('tp'), may hold values from -0.75 to 0.75
- out_large: bfloat16 [2048, 2048], P('tp'), may hold values from -0.75 to 0.75
- gain_one: float32 [2048], replicated, may hold values from 0.1 to 1.9
- shift_one: float32 [2048], replicated, may hold values from -1.5 to 1.5
- gain_two: float32 [2048], replicated, may hold values from 0.1 to 1.9
- shift_two: float32 [2048], replicated, may hold values from -1.5 to 1.5
- expert_pick: int32 [1024, 2], P('sp'), may hold values from 0 to 7, as said below
- route_weight: float32 [1024, 2], P('sp'), may hold values from 0.2 to 1
- w_gate: bfloat16 [8, 2048, 4096], P('sp', None, 'tp'), may hold values from -0.125 to 0.125
- w_up: bfloat16 [8, 2048, 4096], P('sp', None, 'tp'), may hold values from -0.125 to 0.125
- w_down: bfloat16 [8, 4096, 2048], P('sp', 'tp'), may hold values from -0.09375 to 0.09375
Outputs:
- result: bfloat16 [1024, 2048], P(('sp', 'tp'))
Inputs may be any that keep to these rules, and one draw needn't show every extreme that they name: In each aligned block of 128 positions (the positions of one index of sp), no expert is named more than 64 times, and in every block some expert is named exactly 64 times. The two experts of a position differ and lie in one group: equal values of expert_pick // 2.
All inputs are finite; a program needn't handle non-finite values.
Results may differ from a plain program's by a relative error of at most 0.017.
Values may be sent and summed in bfloat16 or wider, within the bound.
A program may use at most 64 MiB of HBM per device.

v0:
```python
import jax
import jax.numpy as jnp
from jax import lax
from jax.sharding import PartitionSpec as P

HEAD_SMALL = 64
HEAD_LARGE = 128


ALPHA_RES = 2.0**0.25
NORM_EPS = 1e-05


def layer_norm(inputs, gain_vec, shift_vec):
    average = jnp.mean(inputs, axis=-1, keepdims=True)
    centred = inputs - average
    variance = jnp.mean(centred * centred, axis=-1, keepdims=True)
    return centred * lax.rsqrt(variance + NORM_EPS) * gain_vec + shift_vec


def stick_group(queries, key_rows, value_rows, log_bias, position):
    query_count = queries.shape[0]
    head_count = queries.shape[1]
    value_size = value_rows.shape[2]
    key_span = 4 * query_count
    score_scale = queries.shape[2] ** (-0.5)
    query_pos = position * query_count + jnp.arange(query_count, dtype=jnp.int32)
    block_count = (position * query_count + query_count + key_span - 1) // key_span

    def visit_block(turn_index, carry):
        running, stay_sum = carry
        first_key = (block_count - 1 - turn_index) * key_span
        key_block = lax.dynamic_slice_in_dim(key_rows, first_key, key_span, 0)
        value_block = lax.dynamic_slice_in_dim(value_rows, first_key, key_span, 0)
        bias_block = lax.dynamic_slice_in_dim(log_bias, first_key, key_span, 0).astype(jnp.float32)
        scores = jnp.einsum("qhd,khd->hqk", queries, key_block, preferred_element_type=jnp.float32)
        scores = scores * score_scale + bias_block.T[:, None, :]
        key_pos = first_key + jnp.arange(key_span, dtype=jnp.int32)
        causal = (key_pos[None, :] < query_pos[:, None])[None]
        log_stay = jnp.where(causal, jax.nn.log_sigmoid(-scores), 0.0)
        later_sum = lax.cumsum(log_stay, axis=2, reverse=True) - log_stay + stay_sum[:, :, None]
        stick_weight = jnp.where(
            causal, jnp.exp(jax.nn.log_sigmoid(scores) + later_sum), 0.0
        ).astype(jnp.bfloat16)
        running = running + jnp.einsum(
            "hqk,khd->qhd", stick_weight, value_block, preferred_element_type=jnp.float32
        )
        stay_sum = stay_sum + jnp.sum(log_stay, axis=2)
        return (running, stay_sum)

    start_total = jnp.zeros((query_count, head_count, value_size), jnp.float32)
    start_stay = jnp.zeros((head_count, query_count), jnp.float32)
    running, stay_sum = lax.fori_loop(0, block_count, visit_block, (start_total, start_stay))
    return running.reshape(query_count, head_count * value_size).astype(jnp.bfloat16)


def split_heads(array, head_size):
    return array.reshape(array.shape[0], array.shape[1] // head_size, head_size)


def local(
    stream,
    query_small,
    key_small,
    value_small,
    query_large,
    key_large,
    value_large,
    key_bias,
    out_small,
    out_large,
    gain_one,
    shift_one,
    gain_two,
    shift_two,
    expert_pick,
    route_weight,
    w_gate,
    w_up,
    w_down,
):
    row_count = stream.shape[0]
    position = lax.axis_index("sp")
    gathered = (
        lax.all_gather(key_small, "sp", axis=0, tiled=True),
        lax.all_gather(value_small, "sp", axis=0, tiled=True),
        lax.all_gather(key_large, "sp", axis=0, tiled=True),
        lax.all_gather(value_large, "sp", axis=0, tiled=True),
        lax.all_gather(key_bias, "sp", axis=0, tiled=True),
    )
    att_small = stick_group(
        split_heads(query_small, HEAD_SMALL),
        split_heads(gathered[0], HEAD_SMALL),
        split_heads(gathered[1], HEAD_SMALL),
        gathered[4][:, 0],
        position,
    )
    att_large = stick_group(
        split_heads(query_large, HEAD_LARGE),
        split_heads(gathered[2], HEAD_LARGE),
        split_heads(gathered[3], HEAD_LARGE),
        gathered[4][:, 1],
        position,
    )
    partial_value = jnp.dot(att_small, out_small, preferred_element_type=jnp.float32)
    partial_value = partial_value + jnp.dot(
        att_large, out_large, preferred_element_type=jnp.float32
    )
    mixer_out = lax.psum(partial_value.astype(jnp.bfloat16), "tp").astype(jnp.float32)
    normed = layer_norm(
        ALPHA_RES * stream.astype(jnp.float32) + mixer_out, gain_one, shift_one
    ).astype(jnp.bfloat16)
    experts = w_gate.shape[0] * lax.axis_size("sp")
    capacity = 4 * row_count // experts
    tp_count = lax.axis_size("tp")
    tp_index = lax.axis_index("tp")
    per_lane = capacity // tp_count
    flat_picks = expert_pick.reshape(-1)
    one_hot = (flat_picks[:, None] == jnp.arange(experts, dtype=jnp.int32)[None, :]).astype(
        jnp.int32
    )
    slot_rank = jnp.sum((jnp.cumsum(one_hot, axis=0) - one_hot) * one_hot, axis=1)
    slot_index = (flat_picks * capacity + slot_rank).reshape(row_count, 2)

    def selector(first_slot, slot_count):
        target = (
            jnp.arange(experts, dtype=jnp.int32)[:, None] * capacity
            + first_slot
            + jnp.arange(slot_count, dtype=jnp.int32)[None, :]
        ).reshape(-1)
        return [target[:, None] == slot_index[None, :, pick_index] for pick_index in range(2)]

    own_select = selector(tp_index * per_lane, per_lane)
    all_select = selector(0, capacity)
    placing = (all_select[0] | all_select[1]).astype(jnp.bfloat16)
    outgoing = jnp.dot(placing, normed, preferred_element_type=jnp.float32).astype(jnp.bfloat16)
    arrived = lax.all_to_all(
        outgoing.reshape(experts, capacity, normed.shape[1]),
        "sp",
        split_axis=0,
        concat_axis=0,
        tiled=True,
    )
    flat_rows = arrived.reshape(-1, arrived.shape[2])
    gate = jnp.dot(flat_rows, w_gate[0], preferred_element_type=jnp.float32)
    upper = jnp.dot(flat_rows, w_up[0], preferred_element_type=jnp.float32)
    hidden = (jax.nn.silu(gate) * upper).astype(jnp.bfloat16)
    expert_terms = jnp.dot(hidden, w_down[0], preferred_element_type=jnp.float32).reshape(
        arrived.shape
    )
    summed = lax.psum_scatter(
        expert_terms.astype(jnp.bfloat16), "tp", scatter_dimension=1, tiled=True
    )
    returned = lax.all_to_all(summed, "sp", split_axis=0, concat_axis=0, tiled=True).reshape(
        experts * per_lane, normed.shape[1]
    )
    picked_first = jnp.einsum(
        "sr,sd->rd",
        own_select[0].astype(jnp.bfloat16),
        returned,
        preferred_element_type=jnp.float32,
    )
    picked_second = jnp.einsum(
        "sr,sd->rd",
        own_select[1].astype(jnp.bfloat16),
        returned,
        preferred_element_type=jnp.float32,
    )
    partial_mix = route_weight[:, 0:1] * picked_first + route_weight[:, 1:2] * picked_second
    expert_mix = lax.psum_scatter(
        partial_mix.astype(jnp.bfloat16), "tp", scatter_dimension=0, tiled=True
    ).astype(jnp.float32)
    own_count = row_count // tp_count
    own_rows = lax.dynamic_slice_in_dim(normed, tp_index * own_count, own_count, 0).astype(
        jnp.float32
    )
    return layer_norm(ALPHA_RES * own_rows + expert_mix, gain_two, shift_two).astype(jnp.bfloat16)


def solution(mesh):
    placed = (
        P("sp", None),
        P("sp", "tp"),
        P("sp", "tp"),
        P("sp", "tp"),
        P("sp", "tp"),
        P("sp", "tp"),
        P("sp", "tp"),
        P("sp", None, "tp"),
        P("tp", None),
        P("tp", None),
        P(),
        P(),
        P(),
        P(),
        P("sp", None),
        P("sp", None),
        P("sp", None, "tp"),
        P("sp", None, "tp"),
        P("sp", "tp", None),
    )
    return jax.shard_map(
        local, mesh=mesh, in_specs=placed, out_specs=P(("sp", "tp"), None), check_vma=False
    )
```

profile of v0, /device:TPU:0, one launch (start us, length us, event | category | flops | bytes accessed | tf_op | source)
XLA Modules:
  0.0 308.8 jit_solution(16901779927208205909)
XLA Ops:
  6.5 0.7 all-gather.3.cloned.1.call-update
  7.3 0.0 all-gather.5.cloned.1.call-start
  7.3 1.7 copy.76
  9.0 0.0 all-reduce.2.cloned.1.call-start
  9.1 13.8 %all_gather.17 = bf16[1024,2,4]{0,2,1:T(4,128)(2,1)S(1)} all-gather(bf16[128,2,4]{0,2,1:T(4,128)(2,1)} %param.30), channel_id=1, replica_groups=mesh['sp'=8,'tp'=4] {'sp'}, dimensions={0}, use_global_device_ids=true | all-gather | bytes 18432 | tf_op jit(solution)/shard_map/all_gather | solution.py:89
  22.9 1.0 copy.74
  23.9 16.5 %all_gather.16 = bf16[1024,256]{1,0:T(8,128)(2,1)S(1)} all-gather(bf16[128,256]{1,0:T(8,128)(2,1)} %param.25), channel_id=1, replica_groups=mesh['sp'=8,'tp'=4] {'sp'}, dimensions={0}, use_global_device_ids=true | all-gather | bytes 589824 | tf_op jit(solution)/shard_map/all_gather | solution.py:85
  40.3 0.2 copy.73
  40.5 16.8 %all_gather.15 = bf16[1024,256]{1,0:T(8,128)(2,1)S(1)} all-gather(bf16[128,256]{1,0:T(8,128)(2,1)S(1)} %copy-done.12), channel_id=1, replica_groups=mesh['sp'=8,'tp'=4] {'sp'}, dimensions={0}, use_global_device_ids=true | all-gather | bytes 589824 | tf_op jit(solution)/shard_map/all_gather | solution.py:86
  57.3 1.0 copy.72
  58.3 10.1 %while.30 = (s32[]{:T(128)}, f32[128,4,64]{0,2,1:T(8,128)S(1)}, f32[4,128]{1,0:T(4,128)S(1)}, s32[]{:T(128)}, s32[]{:T(128)}, /*index=5*/bf16[1024,4,64]{0,2,1:T...) while((s32[]{:T(128)}, f32[128,4,64]{0,2,1:T(8,128)S(1)}, ...), condition=%wide.region_4.5_spmd.clone, body=%wide.region_0.4_spmd.clone.sunk | while | flops 109160584 | bytes 23688592 | solution.py:53
  58.4 0.1 broadcast_compare_fusion.4
  58.6 2.0 fusion.106
  60.5 4.8 %fusion.107 = f32[4,128,4,128]{1,2,3,0:T(4,128)S(1)} fusion(f32[4,128,4,128]{1,3,2,0:T(8,128)S(1)} %bitcast.122), kind=kOutput, calls=%fused_computation.18.clone.1 | output fusion | flops 33292288 | bytes 2097152 | tf_op jit(solution)/shard_map/reduce-window.10
  65.4 0.2 broadcast_add_fusion.5
  65.6 0.1 copy.95
  65.7 0.9 copy-done.1
  66.6 1.5 fusion.108
  68.1 0.2 fusion.109
  68.4 0.1 copy.80
  68.5 0.1 eq.84
  68.7 0.1 eq.80
  68.8 0.1 iota_add_fusion.4
  68.9 0.1 add.323
  69.0 0.6 reduce-window.38
  69.5 0.2 slice_reduce_fusion
  69.8 0.1 copy.77
  69.9 0.1 copy.79
  70.1 2.6 fusion.71
  72.7 2.3 copy.75
  75.0 11.4 %while.31 = (s32[]{:T(128)}, f32[128,4,128]{0,2,1:T(8,128)S(1)}, f32[4,128]{1,0:T(4,128)S(1)}, s32[]{:T(128)}, s32[]{:T(128)}, /*index=5*/bf16[1024,4,128]{0,2,1...) while((s32[]{:T(128)}, f32[128,4,128]{0,2,1:T(8,128)S(1)}, ...), condition=%wide.region_9.10_spmd.clone, body=%wide.region_5.9_spmd.clone.sunk | while | flops 176302208 | bytes 22967640 | solution.py:53
  75.2 0.1 broadcast_compare_fusion.5
  75.4 3.1 fusion.114
  78.4 4.8 %fusion.115 = f32[4,128,4,128]{1,2,3,0:T(4,128)S(1)} fusion(f32[4,128,4,128]{1,3,2,0:T(8,128)S(1)} %bitcast.123), kind=kOutput, calls=%fused_computation.47.clone.1 | output fusion | flops 33292288 | bytes 2097152 | tf_op jit(solution)/shard_map/reduce-window.12
  83.3 0.2 broadcast_add_fusion.6
  83.5 0.1 copy.97
  83.6 0.9 copy-done.2
  84.5 1.5 fusion.116
  86.0 0.3 fusion.117
  86.4 2.5 fusion.50
  89.0 0.0 reduce-scatter.3.cloned.1.call-start
  89.0 0.1 fusion.69
  89.1 0.1 reduce_sum.72
  89.3 0.1 copy.82
  89.4 64.7 %all-reduce.2.cloned.1.call-done = bf16[128,2048]{1,0:T(8,128)(2,1)} async-done(((bf16[128,2048]{1,0:T(8,128)(2,1)}), bf16[128,2048]{1,0:T(8,128)(2,1)}) %all-reduce.2.cloned.1.call-update) | async-done | bytes 524304 | tf_op jit(solution)/shard_map/psum | solution.py:109
  154.1 1.4 fusion.54
  155.4 1.4 multiply_reduce_fusion
  156.8 0.3 add_convert_fusion
  157.2 0.7 convolution_convert_fusion
  157.9 53.7 %all_to_all.10 = bf16[8,64,2048]{2,1,0:T(8,128)(2,1)S(1)} all-to-all(bf16[8,64,2048]{2,1,0:T(8,128)(2,1)S(1)} %bitcast.125), channel_id=1, replica_groups=mesh['sp'=8,'tp'=4] {'sp'}, dimensions={0} | all-to-all | bytes 4194304 | tf_op jit(solution)/shard_map/all_to_all | solution.py:137
  211.7 2.3 fusion.44
  214.0 2.5 multiply_convert_fusion
  216.6 3.7 %fusion.46 = bf16[8,64,2048]{2,1,0:T(8,128)(2,1)} fusion(bf16[8,64,1024]{2,1,0:T(8,128)(2,1)S(1)} %bitcast.137, bf16[1,1024,2048]{2,1,0:T(8,128)(2,1)S(1)} %copy-done.24), kind=kOutput, calls=%fused_computation.66 | convolution fusion | flops 2148532224 | bytes 7340032 | tf_op jit(solution)/shard_map/dot_general | solution.py:148
  220.3 33.3 %reduce-scatter.3.cloned.1.call-done = bf16[8,16,2048]{2,1,0:T(8,128)(2,1)} async-done(((bf16[8,64,2048]{2,1,0:T(8,128)(2,1)}), bf16[8,16,2048]{2,1,0:T(8,128)(2,1)}) %reduce-scatter.3.cloned.1.call-update) | async-done | bytes 524304 | tf_op jit(solution)/shard_map/reduce_scatter | solution.py:151
  253.6 4.6 %all-to-all-start.1 = ((bf16[8,16,2048]{2,1,0:T(8,128)(2,1)}), bf16[8,16,2048]{2,1,0:T(8,128)(2,1)S(1)}, u32[]{:S(2)}, u32[]{:S(2)}) async-start(bf16[8,16,2048]{2,1,0:T(8,128)(2,1)} %reduce-scatter.3.cloned.1.call-done), calls=%async_computation.2 | async-start | bytes 1048576 | tf_op jit(solution)/shard_map/all_to_all | solution.py:154
  258.3 0.1 iota_add_fusion.5
  258.3 0.1 add.318
  258.4 15.1 %all-to-all-done.1 = bf16[8,16,2048]{2,1,0:T(8,128)(2,1)S(1)} async-done(((bf16[8,16,2048]{2,1,0:T(8,128)(2,1)}), bf16[8,16,2048]{2,1,0:T(8,128)(2,1)S(1)}, u32[]{:S(2)}, u32[]{:S(2)}) %all-to-all-start.1) | async-done | bytes 524320 | tf_op jit(solution)/shard_map/all_to_all | solution.py:154
  273.5 0.4 convolution_multiply_fusion.3
  273.9 1.2 fusion.51
  275.2 23.2 %reduce-scatter.5.cloned.1.call-done = bf16[32,2048]{1,0:T(8,128)(2,1)} async-done(((bf16[128,2048]{1,0:T(8,128)(2,1)}), bf16[32,2048]{1,0:T(8,128)(2,1)}) %reduce-scatter.5.cloned.1.call-update) | async-done | bytes 131088 | tf_op jit(solution)/shard_map/reduce_scatter | solution.py:170
  298.4 1.1 fusion.58
  299.4 1.1 multiply_reduce_fusion.1
  300.6 1.7 add_convert_fusion.1
  (90 shorter events, 0.5 us)
Async XLA Ops:
  6.5 79.8 %copy-start = (bf16[512,2048]{1,0:T(8,128)(2,1)S(1)}, bf16[512,2048]{1,0:T(8,128)(2,1)}, u32[]{:S(2)}) copy-start(bf16[512,2048]{1,0:T(8,128)(2,1)} %param.32) | copy-start | bytes 6291460
  6.5 34.0 %copy-start.12 = (bf16[128,256]{1,0:T(8,128)(2,1)S(1)}, bf16[128,256]{1,0:T(8,128)(2,1)}, u32[]{:S(2)}) copy-start(bf16[128,256]{1,0:T(8,128)(2,1)} %param.26) | copy-start | bytes 196612
  6.5 66.1 %all-gather.3.cloned.1.call-start = ((), (), s32[]{:S(2)}) async-start(), calls=%async_computation.4 | async-start | bytes 1179648 | tf_op jit(solution)/shard_map/all_gather | solution.py:88
  7.3 67.7 %all-gather.5.cloned.1.call-start = ((), (), s32[]{:S(2)}) async-start(), calls=%async_computation.5 | async-start | bytes 1179648 | tf_op jit(solution)/shard_map/all_gather | solution.py:87
  9.0 145.1 %all-reduce.2.cloned.1.call-start = ((), (), s32[]{:S(2)}) async-start(), calls=%async_computation.6 | async-start | bytes 1048576 | tf_op jit(solution)/shard_map/psum | solution.py:109
  58.3 10.1 %copy-start.20 = (s32[128,2]{0,1:T(2,128)S(1)}, s32[128,2]{0,1:T(2,128)}, u32[]{:S(2)}) copy-start(s32[128,2]{0,1:T(2,128)} %param.37) | copy-start | bytes 3076
  58.3 11.5 %copy-start.9 = (bf16[128,512]{1,0:T(8,128)(2,1)S(1)}, bf16[128,512]{1,0:T(8,128)(2,1)}, u32[]{:S(2)}) copy-start(bf16[128,512]{1,0:T(8,128)(2,1)} %param.27) | copy-start | bytes 393220
  58.4 2.2 copy-start.7
  58.4 2.2 copy-start.13
  65.4 1.2 copy-start.1
  65.6 2.5 copy-start.4
  66.6 1.7 copy-start.8
  66.6 1.8 copy-start.14
  69.8 5.1 %copy-start.19 = (s32[8,3]{0,1:T(4,128)}, s32[8,3]{0,1:T(4,128)S(1)}, u32[]{:S(2)}) copy-start(s32[8,3]{0,1:T(4,128)S(1)} %reduce-window.39) | copy-start | bytes 292
  75.2 3.3 %copy-start.10 = (bf16[128,4,128]{2,0,1:T(8,128)(2,1)}, bf16[128,4,128]{2,0,1:T(8,128)(2,1)S(1)}, u32[]{:S(2)}) copy-start(bf16[128,4,128]{2,0,1:T(8,128)(2,1)S(1)} %get-tuple-element.581) | copy-start | bytes 393220 | tf_op jit(solution)/shard_map/while
  83.3 1.2 copy-start.2
  83.5 2.5 copy-start.3
  84.5 1.8 copy-start.11
  86.4 2.6 slice-start
  86.4 67.7 %copy-start.5 = (bf16[128,2048]{1,0:T(8,128)(2,1)S(1)}, bf16[128,2048]{1,0:T(8,128)(2,1)}, u32[]{:S(2)}) copy-start(bf16[128,2048]{1,0:T(8,128)(2,1)} %param.23) | copy-start | bytes 1572868
  88.9 67.9 %copy-start.15 = (f32[2048]{0:T(1024)S(1)}, f32[2048]{0:T(1024)}, u32[]{:S(2)}) copy-start(f32[2048]{0:T(1024)} %param.34) | copy-start | bytes 24580
  89.0 67.9 %copy-start.16 = (f32[2048]{0:T(1024)S(1)}, f32[2048]{0:T(1024)}, u32[]{:S(2)}) copy-start(f32[2048]{0:T(1024)} %param.33) | copy-start | bytes 24580
  89.0 164.6 %reduce-scatter.3.cloned.1.call-start = ((), (), s32[]{:S(2)}) async-start(), calls=%async_computation.7 | async-start | bytes 2621440 | tf_op jit(solution)/shard_map/reduce_scatter | solution.py:151
  154.1 2.8 copy-start.6
  157.9 53.7 %copy-start.22 = (bf16[1,2048,1024]{2,1,0:T(8,128)(2,1)S(1)}, bf16[1,2048,1024]{2,1,0:T(8,128)(2,1)}, u32[]{:S(2)}) copy-start(bf16[1,2048,1024]{2,1,0:T(8,128)(2,1)} %param.39) | copy-start | bytes 12582916
  211.6 2.4 copy-start.23
  214.0 2.5 copy-start.24
  220.3 38.1 %copy-start.21 = (f32[128,2]{0,1:T(2,128)S(1)}, f32[128,2]{0,1:T(2,128)}, u32[]{:S(2)}) copy-start(f32[128,2]{0,1:T(2,128)} %param.38) | copy-start | bytes 3076
  253.6 19.9 %all-to-all-start.1 = ((bf16[8,16,2048]{2,1,0:T(8,128)(2,1)}), bf16[8,16,2048]{2,1,0:T(8,128)(2,1)S(1)}, u32[]{:S(2)}, u32[]{:S(2)}) async-start(bf16[8,16,2048]{2,1,0:T(8,128)(2,1)} %reduce-scatter.3.cloned.1.call-done), calls=%async_computation.2 | async-start | bytes 1048576 | tf_op jit(solution)/shard_map/all_to_all | solution.py:154
  258.2 40.2 %reduce-scatter.5.cloned.1.call-start = ((), (), s32[]{:S(2)}) async-start(), calls=%async_computation.8 | async-start | bytes 655360 | tf_op jit(solution)/shard_map/reduce_scatter | solution.py:170
  273.5 27.0 %copy-start.17 = (f32[2048]{0:T(1024)S(1)}, f32[2048]{0:T(1024)}, u32[]{:S(2)}) copy-start(f32[2048]{0:T(1024)} %param.36) | copy-start | bytes 24580
  273.5 27.1 %copy-start.18 = (f32[2048]{0:T(1024)S(1)}, f32[2048]{0:T(1024)}, u32[]{:S(2)}) copy-start(f32[2048]{0:T(1024)} %param.35) | copy-start | bytes 24580
Sparse Core Ops, SparseCore 0:
  8.9 27.5 all-gather.2
  38.1 26.5 all-gather.4
  89.1 64.9 all-reduce.1
  220.4 33.1 reduce-scatter.2
  275.3 23.0 reduce-scatter.4
where the time goes:
time: 309 us
  waiting for transfers between devices  137 us (44%)
  blocking collectives  101 us (33%)
  matrix products  21.6 us (7%)
  other arithmetic  21.1 us (7%)
  between operations  13.4 us (4%)
  local copies, waits for them, and re-layouts  9.51 us (3%)
  starting transfers between devices  4.77 us (2%)
    psum x1, waiting for transfers between devices, local(): lax.psum(partial_value.astype(jnp.bfloat16), 'tp').astype(jnp.float32)  64.7 us
    all_to_all x1, blocking collectives, local(): lax.all_to_all(outgoing.reshape(experts, capacity, normed.shape[1]), 'sp'...  53.7 us
    reduce_scatter x1, waiting for transfers between devices, local(): lax.psum_scatter(expert_terms.astype(jnp.bfloat16), 'tp', scatter_dimensi...  33.3 us
    reduce_scatter x1, waiting for transfers between devices, local(): lax.psum_scatter(partial_mix.astype(jnp.bfloat16), 'tp', scatter_dimensio...  23.2 us
    all_gather x1, blocking collectives, local(): lax.all_gather(value_small, 'sp', axis=0, tiled=True)  16.8 us
    all_gather x1, blocking collectives, local(): lax.all_gather(key_small, 'sp', axis=0, tiled=True)  16.5 us
    all_to_all x1, waiting for transfers between devices, local(): lax.all_to_all(summed, 'sp', split_axis=0, concat_axis=0, tiled=True)  15.1 us
    all_gather x1, blocking collectives, local(): lax.all_gather(key_bias, 'sp', axis=0, tiled=True)  13.8 us
  transfers between devices with their start and end apart: 6, of which 4 were waited for; matrix products, arithmetic and copies ran while one was open for 6% of the time, Pallas kernels for 0%

commit v1 on v0

--- a/solution.py
+++ b/solution.py
@@ -1,6 +1,10 @@
+import functools
+
 import jax
 import jax.numpy as jnp
 from jax import lax
+from jax.experimental import pallas as pl
+from jax.experimental.pallas import tpu as pltpu
 from jax.sharding import PartitionSpec as P
 
 HEAD_SMALL = 64
@@ -177,6 +181,471 @@
     return layer_norm(ALPHA_RES * own_rows + expert_mix, gain_two, shift_two).astype(jnp.bfloat16)
 
 
+GROUPS = 4
+
+
+def fast_kernel(
+    dims,
+    qs_ref, ks_ref, vs_ref, ql_ref, kl_ref, vl_ref, bias_ref, stream_ref, os_ref, ol_ref,
+    g1_ref, b1_ref, g2_ref, b2_ref, pick_ref, route_ref, wg_ref, wu_ref, wd_ref,
+    out_ref,
+    pack_a, pack_v, rq, rk, rv, rb, aq, ak, ao, ra, wos, wol, strm, pb, rp, st, rst, normed,
+    place, xs, wsend, wrecv, ag, wg, wu, wd, hid, own_y, cs, cr, ts, rr, zs, zr, fs, fr,
+    load_sem, q_send, q_recv, a_send, a_recv, p_send, p_recv, s_send, s_recv,
+    x_send, x_recv, w_send, w_recv, g_send, g_recv, h_send, h_recv, c_send, c_recv,
+    t_send, t_recv, z_send, z_recv, f_send, f_recv,
+):
+    n_sp, n_tp, rows, cols, cap, small_heads, hs, hl = dims
+    f32, bf16 = jnp.float32, jnp.bfloat16
+    sp = lax.axis_index("sp")
+    tp = lax.axis_index("tp")
+    core = lax.rem(sp, 2)
+    chip = lax.div(sp, 2)
+    sibling = sp + 1 - 2 * core
+    n_z = n_sp // 2
+    is_small = sp < small_heads
+    large_heads = n_sp - small_heads
+    ffw = wg_ref.shape[2]
+    width = n_tp * cols
+
+    def mesh_copy(src, dst, send, recv, target):
+        return pltpu.make_async_remote_copy(
+            src_ref=src, dst_ref=dst, send_sem=send, recv_sem=recv,
+            device_id=target, device_id_type=pl.DeviceIdType.MESH,
+        )
+
+    def sp_at(j):
+        return (j, tp)
+
+    def tp_at(j):
+        return (sp, j)
+
+    barrier = pltpu.get_barrier_semaphore()
+    for k in range(1, n_sp):
+        pl.semaphore_signal(barrier, inc=1, device_id=sp_at(lax.rem(sp + k, n_sp)), device_id_type=pl.DeviceIdType.MESH)
+    for k in range(1, n_tp):
+        pl.semaphore_signal(barrier, inc=1, device_id=tp_at(lax.rem(tp + k, n_tp)), device_id_type=pl.DeviceIdType.MESH)
+
+    own_cols = pl.ds(pl.multiple_of(tp * cols, cols), cols)
+    loads = [
+        pltpu.make_async_copy(os_ref, wos, load_sem.at[0]),
+        pltpu.make_async_copy(ol_ref, wol, load_sem.at[1]),
+        pltpu.make_async_copy(stream_ref.at[:, own_cols], strm, load_sem.at[2]),
+        pltpu.make_async_copy(wg_ref.at[0], wg, load_sem.at[3]),
+        pltpu.make_async_copy(wu_ref.at[0], wu, load_sem.at[4]),
+        pltpu.make_async_copy(wd_ref.at[0], wd, load_sem.at[5]),
+    ]
+    for load in loads:
+        load.start()
+
+    for h in range(small_heads):
+        part = slice(h * hs, (h + 1) * hs)
+        pack_a[h] = jnp.concatenate([qs_ref[:, part], ks_ref[:, part]], axis=1)
+        pack_v[h] = jnp.concatenate([vs_ref[:, part], jnp.zeros((rows, hl - hs), bf16)], axis=1)
+
+    pl.semaphore_wait(barrier, n_sp + n_tp - 2)
+
+    def head_copies(j, slot):
+        if j < small_heads:
+            pairs = [(0, pack_a.at[j], rq), (2, pack_v.at[j], rv)]
+        else:
+            part = pl.ds((j - small_heads) * hl, hl)
+            pairs = [(0, ql_ref.at[:, part], rq), (1, kl_ref.at[:, part], rk), (2, vl_ref.at[:, part], rv)]
+        pairs.append((3, bias_ref.at[j], rb))
+        return [(kind, src, dst.at[slot]) for kind, src, dst in pairs]
+
+    for j in range(n_sp):
+        @pl.when(j != sp)
+        def _():
+            for kind, src, dst in head_copies(j, sp):
+                mesh_copy(src, dst, q_send.at[kind, j], q_recv.at[kind, sp], sp_at(j)).start()
+
+        @pl.when(j == sp)
+        def _():
+            for kind, src, dst in head_copies(j, j):
+                pltpu.make_async_copy(src, dst, q_recv.at[kind, j]).start()
+
+    group = lax.div(pick_ref[0:1, :], 2)
+    first_even = lax.rem(pick_ref[0:1, :], 2) == 0
+    sub8 = lax.broadcasted_iota(jnp.int32, (8, rows), 0)
+    one_hot = (sub8 == group).astype(f32)
+    sub_r = lax.broadcasted_iota(jnp.int32, (rows, rows), 0)
+    lane_r = lax.broadcasted_iota(jnp.int32, (rows, rows), 1)
+    before = (sub_r < lane_r).astype(f32).astype(bf16)
+    counts = jnp.dot(one_hot.astype(bf16), before, preferred_element_type=f32)
+    rank = jnp.sum(one_hot * counts, axis=0, keepdims=True).astype(jnp.int32)
+    slot_row = group * cap + rank
+    slot_iota = lax.broadcasted_iota(jnp.int32, (GROUPS * cap, rows), 0)
+    place[...] = (slot_iota == slot_row).astype(f32).astype(bf16)
+    w_even = jnp.where(first_even, route_ref[0:1, :], route_ref[1:2, :])
+    w_odd = jnp.where(first_even, route_ref[1:2, :], route_ref[0:1, :])
+    w8 = jnp.where(sub8 == 0, w_even, jnp.where(sub8 == 1, w_odd, 0.0))
+    w_hi = w8.astype(bf16)
+    w_lo = (w8 - w_hi.astype(f32)).astype(bf16)
+    for g in range(GROUPS):
+        pick_g = ((sub_r == slot_row - g * cap) & (sub_r < cap)).astype(f32).astype(bf16)
+        last = (((1,), (1,)), ((), ()))
+        wsend[g] = lax.dot_general(w_hi, pick_g, last, preferred_element_type=f32) + lax.dot_general(
+            w_lo, pick_g, last, preferred_element_type=f32
+        )
+
+    for j in range(n_sp):
+        for kind in (0, 2, 3):
+            dst = (rq, None, rv, rb)[kind].at[j]
+            pltpu.make_async_copy(dst, dst, q_recv.at[kind, j]).wait()
+
+    @pl.when(jnp.logical_not(is_small))
+    def _():
+        for j in range(n_sp):
+            pltpu.make_async_copy(rk.at[j], rk.at[j], q_recv.at[1, j]).wait()
+            aq[pl.ds(j * rows, rows), :] = rq[j]
+            ak[pl.ds(j * rows, rows), :] = rk[j]
+
+    @pl.when(is_small)
+    def _():
+        lane = lax.broadcasted_iota(jnp.int32, (rows, hl), 1)
+        for j in range(n_sp):
+            both = rq[j]
+            aq[pl.ds(j * rows, rows), :] = jnp.where(lane < hs, both, jnp.zeros_like(both))
+            ak[pl.ds(j * rows, rows), :] = jnp.concatenate([both[:, hs:], both[:, :hs]], axis=1)
+
+    for j in range(n_sp):
+        @pl.when(j != sp)
+        def _():
+            for kind, src, dst in head_copies(j, sp):
+                mesh_copy(src, dst, q_send.at[kind, j], q_recv.at[kind, sp], sp_at(j)).wait_send()
+
+    scale = jnp.where(is_small, hs**-0.5, hl**-0.5).astype(f32)
+    span = 2 * rows
+    sub_t = lax.broadcasted_iota(jnp.int32, (span, span), 0)
+    lane_t = lax.broadcasted_iota(jnp.int32, (span, span), 1)
+    tri = (sub_t >= lane_t).astype(f32).astype(bf16)
+    causal = lane_t < sub_t
+
+    def tile(query, kj, diagonal, total, later):
+        keys = ak[pl.ds(pl.multiple_of(kj * span, span), span), :]
+        log_odds = jnp.concatenate([rb[2 * kj, 0:1, :], rb[2 * kj + 1, 0:1, :]], axis=1)
+        score = lax.dot_general(query, keys, (((1,), (1,)), ((), ())), preferred_element_type=f32)
+        score = score * scale + log_odds
+        soft = jnp.maximum(score, 0.0) + jnp.log(1.0 + jnp.exp(-jnp.abs(score)))
+        if diagonal:
+            soft = jnp.where(causal, soft, 0.0)
+        high = soft.astype(bf16)
+        low = (soft - high.astype(f32)).astype(bf16)
+        run = jnp.dot(high, tri, preferred_element_type=f32) + jnp.dot(low, tri, preferred_element_type=f32)
+        stick = jnp.exp(score - run - later)
+        if diagonal:
+            stick = jnp.where(causal, stick, 0.0)
+        values = jnp.concatenate([rv[2 * kj], rv[2 * kj + 1]], axis=0)
+        total = total + jnp.dot(stick.astype(bf16), values, preferred_element_type=f32)
+        return total, later + run[:, 0:1]
+
+    for qi in range(n_sp // 2):
+        query = aq[qi * span:(qi + 1) * span, :]
+        carry = tile(query, qi, True, jnp.zeros((span, hl), f32), jnp.zeros((span, 1), f32))
+        if qi:
+            def visit(turn, carry):
+                return tile(query, qi - 1 - turn, False, *carry)
+            carry = lax.fori_loop(0, qi, visit, carry)
+        for half in range(2):
+            d = 2 * qi + half
+            ao[d] = carry[0][half * rows:(half + 1) * rows].astype(bf16)
+        for half in range(2):
+            d = 2 * qi + half
+
+            @pl.when(d != sp)
+            def _():
+                mesh_copy(ao.at[d], ra.at[sp], a_send.at[d], a_recv.at[sp], sp_at(d)).start()
+
+            @pl.when(d == sp)
+            def _():
+                pltpu.make_async_copy(ao.at[d], ra.at[d], a_recv.at[d]).start()
+
+    for load in loads[:3]:
+        load.wait()
+    for j in range(n_sp):
+        pltpu.make_async_copy(ra.at[j], ra.at[j], a_recv.at[j]).wait()
+    att_small = jnp.concatenate([ra[j][:, :hs] for j in range(small_heads)], axis=1)
+    att_large = jnp.concatenate([ra[j] for j in range(small_heads, n_sp)], axis=1)
+
+    def tp_wait_recv(buf, sem, src):
+        pltpu.make_async_copy(buf.at[src], buf.at[src], sem.at[src]).wait()
+
+    for k in range(1, n_tp + 1):
+        t = lax.rem(tp + k, n_tp)
+        part = pl.ds(pl.multiple_of(t * cols, cols), cols)
+        term = jnp.dot(att_small, wos[:, part], preferred_element_type=f32)
+        term = term + jnp.dot(att_large, wol[:, part], preferred_element_type=f32)
+        pb[k - 1] = term.astype(bf16)
+        if k < n_tp:
+            mesh_copy(pb.at[k - 1], rp.at[tp], p_send.at[k], p_recv.at[tp], tp_at(t)).start()
+    mixed = ALPHA_RES * strm[...].astype(f32) + pb[n_tp - 1].astype(f32)
+    for k in range(1, n_tp):
+        src = lax.rem(tp + k, n_tp)
+        tp_wait_recv(rp, p_recv, src)
+        mixed = mixed + rp[src].astype(f32)
+
+    eye = sub_r == lane_r
+
+    def to_row(column):
+        return jnp.sum(jnp.where(eye, column, 0.0), axis=0, keepdims=True)
+
+    def to_column(row):
+        return jnp.sum(jnp.where(eye, row, 0.0), axis=1, keepdims=True)
+
+    own_mean = jnp.mean(mixed, axis=1, keepdims=True)
+    centred = mixed - own_mean
+    own_square = jnp.sum(centred * centred, axis=1, keepdims=True)
+    mean_row, square_row = to_row(own_mean), to_row(own_square)
+    st[...] = jnp.where(sub8 == 0, mean_row, square_row)
+    for k in range(1, n_tp):
+        t = lax.rem(tp + k, n_tp)
+        mesh_copy(st, rst.at[tp], s_send.at[k], s_recv.at[tp], tp_at(t)).start()
+    means, squares = [mean_row], [square_row]
+    for k in range(1, n_tp):
+        src = lax.rem(tp + k, n_tp)
+        tp_wait_recv(rst, s_recv, src)
+        means.append(rst[src, 0:1, :])
+        squares.append(rst[src, 1:2, :])
+    full_mean = sum(means) / n_tp
+    spread = sum(squares) + cols * sum((m - full_mean) * (m - full_mean) for m in means)
+    scale_row = lax.rsqrt(spread / width + NORM_EPS)
+    norm_val = (mixed - to_column(full_mean)) * to_column(scale_row) * g1_ref[:, own_cols] + b1_ref[:, own_cols]
+    normed[...] = norm_val.astype(bf16)
+
+    for g in range(GROUPS):
+        xs[g] = jnp.dot(place[g * cap:(g + 1) * cap, :], normed[...], preferred_element_type=f32).astype(bf16)
+    for k in range(n_z):
+        g = lax.rem(chip + k, n_z)
+        dst = ag.at[core, tp, chip]
+        if k == 0:
+            pltpu.make_async_copy(xs.at[g], dst, x_recv.at[chip]).start()
+        else:
+            mesh_copy(xs.at[g], dst, x_send.at[k], x_recv.at[chip], sp_at(2 * g + core)).start()
+    for k in range(n_sp):
+        j = lax.rem(sp + k, n_sp)
+        if k == 0:
+            pltpu.make_async_copy(wsend.at[chip], wrecv.at[sp], w_recv.at[sp]).start()
+        else:
+            mesh_copy(wsend.at[lax.div(j, 2)], wrecv.at[sp], w_send.at[k], w_recv.at[sp], sp_at(j)).start()
+
+    for k in range(n_z):
+        z = lax.rem(chip + k, n_z)
+        piece = ag.at[core, tp, z]
+        pltpu.make_async_copy(piece, piece, x_recv.at[z]).wait()
+        for m in range(1, n_tp):
+            t = lax.rem(tp + m, n_tp)
+            mesh_copy(piece, piece, g_send.at[m, z], g_recv.at[tp, z], tp_at(t)).start()
+        mesh_copy(piece, piece, h_send.at[tp, z], h_recv.at[tp, z], sp_at(sibling)).start()
+    for load in loads[3:]:
+        load.wait()
+    for k in range(n_z):
+        z = lax.rem(chip + k, n_z)
+        for m in range(1, n_tp):
+            t = lax.rem(tp + m, n_tp)
+            piece = ag.at[core, t, z]
+            pltpu.make_async_copy(piece, piece, g_recv.at[t, z]).wait()
+            mesh_copy(piece, piece, h_send.at[t, z], h_recv.at[t, z], sp_at(sibling)).start()
+
+    half_rows = n_z * cap
+    lane_c = lax.broadcasted_iota(jnp.int32, (cap, rows), 1)
+    sub_c = lax.broadcasted_iota(jnp.int32, (cap, rows), 0)
+    for j in range(n_sp):
+        pltpu.make_async_copy(wrecv.at[j], wrecv.at[j], w_recv.at[j]).wait()
+
+    def slot_weights(c):
+        parts = []
+        for z in range(n_z):
+            row = wrecv[2 * z + c, pl.ds(core, 1), :]
+            parts.append(jnp.sum(jnp.where(sub_c == lane_c, row, 0.0), axis=1, keepdims=True))
+        return jnp.concatenate(parts, axis=0)
+
+    def up_proj(c):
+        step = min(256, ffw)
+
+        def body(n, carry):
+            part = pl.ds(pl.multiple_of(n * step, step), step)
+            gate = jnp.zeros((half_rows, step), f32)
+            upper = jnp.zeros((half_rows, step), f32)
+            for t in range(n_tp):
+                x = ag[c, t].reshape(half_rows, cols)
+                gate = gate + jnp.dot(x, wg[t * cols:(t + 1) * cols, part], preferred_element_type=f32)
+                upper = upper + jnp.dot(x, wu[t * cols:(t + 1) * cols, part], preferred_element_type=f32)
+            hid[:, part] = (gate / (1.0 + jnp.exp(-gate)) * upper).astype(bf16)
+            return carry
+
+        lax.fori_loop(0, ffw // step, body, 0)
+
+    def down_proj(t, weights):
+        part = pl.ds(pl.multiple_of(t * cols, cols), cols)
+        return jnp.dot(hid[...], wd[:, part], preferred_element_type=f32) * weights
+
+    other = 1 - core
+    up_proj(core)
+    own_weights = slot_weights(core)
+    for k in range(1, n_tp + 1):
+        t = lax.rem(tp + k, n_tp)
+        own_y[k - 1] = down_proj(t, own_weights)
+    for t in range(n_tp):
+        for z in range(n_z):
+            piece = ag.at[other, t, z]
+            pltpu.make_async_copy(piece, piece, h_recv.at[t, z]).wait()
+    up_proj(other)
+    other_weights = slot_weights(other)
+    for k in range(1, n_tp + 1):
+        t = lax.rem(tp + k, n_tp)
+        cs[k - 1] = down_proj(t, other_weights).astype(bf16)
+        mesh_copy(cs.at[k - 1], cr.at[k - 1], c_send.at[k - 1], c_recv.at[k - 1], sp_at(sibling)).start()
+    summed = None
+    for k in range(1, n_tp + 1):
+        t = lax.rem(tp + k, n_tp)
+        pltpu.make_async_copy(cr.at[k - 1], cr.at[k - 1], c_recv.at[k - 1]).wait()
+        both = own_y[k - 1] + cr[k - 1].astype(f32)
+        if k < n_tp:
+            ts[k - 1] = both.astype(bf16)
+            mesh_copy(ts.at[k - 1], rr.at[tp], t_send.at[k], t_recv.at[tp], tp_at(t)).start()
+        else:
+            own_y[k - 1] = both
+    for k in range(1, n_tp):
+        tp_wait_recv(rr, t_recv, lax.rem(tp + k, n_tp))
+    for k in range(1, n_z + 1):
+        z = lax.rem(chip + k, n_z)
+        part = pl.ds(pl.multiple_of(z * cap, cap), cap)
+        total = own_y[n_tp - 1, part, :]
+        for m in range(1, n_tp):
+            total = total + rr[lax.rem(tp + m, n_tp), part, :].astype(f32)
+        zs[k - 1] = total.astype(bf16)
+        if k < n_z:
+            mesh_copy(zs.at[k - 1], zr.at[chip], z_send.at[k], z_recv.at[chip], sp_at(2 * z + core)).start()
+        else:
+            pltpu.make_async_copy(zs.at[k - 1], zr.at[chip], z_recv.at[chip]).start()
+    for z in range(n_z):
+        pltpu.make_async_copy(zr.at[z], zr.at[z], z_recv.at[z]).wait()
+    expert_mix = lax.dot_general(
+        place[...], zr[...].reshape(n_z * cap, cols), (((0,), (0,)), ((), ())), preferred_element_type=f32
+    )
+    final = ALPHA_RES * normed[...].astype(f32) + expert_mix
+    own_rows = rows // n_tp
+    for t in range(n_tp):
+        fs[t] = final[t * own_rows:(t + 1) * own_rows]
+    for k in range(1, n_tp):
+        t = lax.rem(tp + k, n_tp)
+        mesh_copy(fs.at[t], fr.at[tp], f_send.at[k], f_recv.at[tp], tp_at(t)).start()
+    keep = pltpu.make_async_copy(fs.at[tp], fr.at[tp], f_recv.at[tp])
+    keep.start()
+    for t in range(n_tp):
+        tp_wait_recv(fr, f_recv, t)
+    blocks = [fr[t] for t in range(n_tp)]
+    average = sum(jnp.sum(b, axis=1, keepdims=True) for b in blocks) / width
+    blocks = [b - average for b in blocks]
+    variance = sum(jnp.sum(b * b, axis=1, keepdims=True) for b in blocks) / width
+    inverse = lax.rsqrt(variance + NORM_EPS)
+    for t in range(n_tp):
+        part = slice(t * cols, (t + 1) * cols)
+        out_ref[:, part] = (blocks[t] * inverse * g2_ref[:, part] + b2_ref[:, part]).astype(bf16)
+
+    for d in range(n_sp):
+        @pl.when(d != sp)
+        def _():
+            mesh_copy(ao.at[d], ra.at[sp], a_send.at[d], a_recv.at[sp], sp_at(d)).wait_send()
+    for k in range(1, n_sp):
+        j = lax.rem(sp + k, n_sp)
+        mesh_copy(wsend.at[lax.div(j, 2)], wrecv.at[sp], w_send.at[k], w_recv.at[sp], sp_at(j)).wait_send()
+    for k in range(1, n_tp):
+        t = lax.rem(tp + k, n_tp)
+        mesh_copy(pb.at[k - 1], rp.at[tp], p_send.at[k], p_recv.at[tp], tp_at(t)).wait_send()
+        mesh_copy(st, rst.at[tp], s_send.at[k], s_recv.at[tp], tp_at(t)).wait_send()
+        mesh_copy(ts.at[k - 1], rr.at[tp], t_send.at[k], t_recv.at[tp], tp_at(t)).wait_send()
+        mesh_copy(fs.at[t], fr.at[tp], f_send.at[k], f_recv.at[tp], tp_at(t)).wait_send()
+        for z in range(n_z):
+            piece = ag.at[core, tp, z]
+            mesh_copy(piece, piece, g_send.at[k, z], g_recv.at[tp, z], tp_at(t)).wait_send()
+    for k in range(1, n_z):
+        g = lax.rem(chip + k, n_z)
+        mesh_copy(xs.at[g], ag.at[core, tp, chip], x_send.at[k], x_recv.at[chip], sp_at(2 * g + core)).wait_send()
+        mesh_copy(zs.at[k - 1], zr.at[chip], z_send.at[k], z_recv.at[chip], sp_at(2 * g + core)).wait_send()
+    for t in range(n_tp):
+        mesh_copy(cs.at[t], cr.at[t], c_send.at[t], c_recv.at[t], sp_at(sibling)).wait_send()
+        for z in range(n_z):
+            piece = ag.at[core, t, z]
+            mesh_copy(piece, piece, h_send.at[t, z], h_recv.at[t, z], sp_at(sibling)).wait_send()
+
+
+def fast_local(
+    stream, query_small, key_small, value_small, query_large, key_large, value_large, key_bias,
+    out_small, out_large, gain_one, shift_one, gain_two, shift_two, expert_pick, route_weight,
+    w_gate, w_up, w_down,
+):
+    f32, bf16 = jnp.float32, jnp.bfloat16
+    n_sp, n_tp = lax.axis_size("sp"), lax.axis_size("tp")
+    rows, width = stream.shape
+    cols = width // n_tp
+    hs, hl = HEAD_SMALL, HEAD_LARGE
+    small_heads = query_small.shape[1] // hs
+    cap = 4 * rows // (w_gate.shape[0] * n_sp)
+    n_z = n_sp // 2
+    ffw = w_gate.shape[2]
+    bias = key_bias.astype(f32).transpose(1, 2, 0).reshape(n_sp, 1, rows)
+    bias = jnp.broadcast_to(bias, (n_sp, 8, rows))
+    vmem = pl.BlockSpec(memory_space=pltpu.VMEM)
+    hbm = pl.BlockSpec(memory_space=pl.ANY)
+    dma = pltpu.SemaphoreType.DMA
+    V = pltpu.VMEM
+    half = n_z * cap
+    scratch = [
+        V((small_heads, rows, hl), bf16), V((small_heads, rows, hl), bf16),
+        V((n_sp, rows, hl), bf16), V((n_sp, rows, hl), bf16), V((n_sp, rows, hl), bf16),
+        V((n_sp, 8, rows), f32),
+        V((n_sp * rows, hl), bf16), V((n_sp * rows, hl), bf16),
+        V((n_sp, rows, hl), bf16), V((n_sp, rows, hl), bf16),
+        V(out_small.shape, bf16), V(out_large.shape, bf16), V((rows, cols), bf16),
+        V((n_tp, rows, cols), bf16), V((n_tp, rows, cols), bf16),
+        V((8, rows), f32), V((n_tp, 8, rows), f32), V((rows, cols), bf16),
+        V((GROUPS * cap, rows), bf16), V((GROUPS, cap, cols), bf16),
+        V((GROUPS, 8, rows), f32), V((n_sp, 8, rows), f32),
+        V((2, n_tp, n_z, cap, cols), bf16),
+        V((width, ffw), bf16), V((width, ffw), bf16), V((ffw, width), bf16),
+        V((half, ffw), bf16), V((n_tp, half, cols), f32),
+        V((n_tp, half, cols), bf16), V((n_tp, half, cols), bf16),
+        V((n_tp, half, cols), bf16), V((n_tp, half, cols), bf16),
+        V((n_z, cap, cols), bf16), V((n_z, cap, cols), bf16),
+        V((n_tp, rows // n_tp, cols), f32), V((n_tp, rows // n_tp, cols), f32),
+        dma((6,)), dma((4, n_sp)), dma((4, n_sp)), dma((n_sp,)), dma((n_sp,)),
+        dma((n_tp,)), dma((n_tp,)), dma((n_tp,)), dma((n_tp,)),
+        dma((n_z,)), dma((n_z,)), dma((n_sp,)), dma((n_sp,)),
+        dma((n_tp, n_z)), dma((n_tp, n_z)), dma((n_tp, n_z)), dma((n_tp, n_z)),
+        dma((n_tp,)), dma((n_tp,)), dma((n_tp,)), dma((n_tp,)),
+        dma((n_z,)), dma((n_z,)), dma((n_tp,)), dma((n_tp,)),
+    ]
+    dims = (n_sp, n_tp, rows, cols, cap, small_heads, hs, hl)
+    return pl.pallas_call(
+        functools.partial(fast_kernel, dims),
+        out_shape=jax.ShapeDtypeStruct((rows // n_tp, width), bf16),
+        in_specs=[vmem] * 7 + [hbm] * 3 + [vmem] * 6 + [hbm] * 3,
+        out_specs=vmem,
+        scratch_shapes=scratch,
+        compiler_params=pltpu.CompilerParams(
+            collective_id=0, has_side_effects=True, vmem_limit_bytes=60 * 1024 * 1024
+        ),
+        name="layer",
+    )(
+        query_small, key_small, value_small, query_large, key_large, value_large, bias,
+        stream, out_small, out_large,
+        gain_one[None], shift_one[None], gain_two[None], shift_two[None],
+        expert_pick.T, route_weight.T, w_gate, w_up, w_down,
+    )
+
+
+def layer(*arrays):
+    n_sp, n_tp = lax.axis_size("sp"), lax.axis_size("tp")
+    heads = arrays[1].shape[1] // HEAD_SMALL + arrays[4].shape[1] // HEAD_LARGE
+    experts = arrays[16].shape[0] * n_sp
+    paired = experts == 2 * GROUPS and n_sp == experts
+    if paired and heads == n_sp and arrays[7].shape[2] * 2 == n_sp and arrays[0].shape[1] % (128 * n_tp) == 0:
+        return fast_local(*arrays)
+    return local(*arrays)
+
+
 def solution(mesh):
     placed = (
         P("sp", None),
@@ -200,5 +669,5 @@
         P("sp", "tp", None),
     )
     return jax.shard_map(
-        local, mesh=mesh, in_specs=placed, out_specs=P(("sp", "tp"), None), check_vma=False
-    )
+        layer, mesh=mesh, in_specs=placed, out_specs=P(("sp", "tp"), None), check_vma=False
+    )

time: 309 us -> 102 us (0.33)
  waiting for transfers between devices: 137 us -> 0 us
  blocking collectives: 101 us -> 0 us
  Pallas kernels: 0 us -> 98.5 us
  matrix products: 21.6 us -> 0 us
  other arithmetic: 21.1 us -> 0.68 us
  between operations: 13.4 us -> 0.01 us
  local copies, waits for them, and re-layouts: 9.51 us -> 2.19 us
  starting transfers between devices: 4.77 us -> 0 us
    pallas_call x0 -> x1, Pallas kernels: none -> 98.5 us  [fast_local(): pl.pallas_call(functools.partial(fast_kernel, dims), out_shape=jax.ShapeD...]
    psum x1 -> x0, waiting for transfers between devices: 64.7 us -> none  [local(): lax.psum(partial_value.astype(jnp.bfloat16), 'tp').astype(jnp.float32)]
    reduce_scatter x2 -> x0, waiting for transfers between devices: 56.5 us -> none  [the longest x1 33.3 us: local(): lax.psum_scatter(expert_terms.astype(jnp.bfloat16), 'tp', scatter_dimensi...]
    all_to_all x1 -> x0, blocking collectives: 53.7 us -> none  [local(): lax.all_to_all(outgoing.reshape(experts, capacity, normed.shape[1]), 'sp'...]
    all_gather x3 -> x0, blocking collectives: 47.1 us -> none  [the longest x1 16.8 us: local(): lax.all_gather(value_small, 'sp', axis=0, tiled=True)]
    dot_general x12 -> x0, matrix products: 21.6 us -> none  [the longest x2 5.02 us: visit_block(): jnp.einsum('qhd,khd->hqk', queries, key_block, preferred_element_type=jnp...]
    all_to_all x1 -> x0, waiting for transfers between devices: 15.1 us -> none  [local(): lax.all_to_all(summed, 'sp', split_axis=0, concat_axis=0, tiled=True)]
    another operation x8 -> x0, other arithmetic: 10.6 us -> none
  transfers between devices with their start and end apart: 6 -> 0, of which waited for: 4 -> 0; matrix products, arithmetic and copies ran while one was open for 6% -> 0% of each run, Pallas kernels for 0% -> 0%
where the time goes in v1:
time: 102 us; the launch traced here: 101 us
  Pallas kernels  98.5 us (97%)
  local copies, waits for them, and re-layouts  2.19 us (2%)
    pallas_call x1, Pallas kernels, fast_local(): pl.pallas_call(functools.partial(fast_kernel, dims), out_shape=jax.ShapeD...  98.5 us

profile of v1, /device:TPU:0, one launch (start us, length us, event | category | flops | bytes accessed | tf_op | source)
XLA Modules:
  0.0 101.4 jit_solution(10663587092336491168)
XLA Ops:
  0.0 0.7 broadcast_in_dim.30
  0.7 0.6 broadcast_in_dim.24.bias_ref
  1.3 98.5 %layer.1 = bf16[32,2048]{1,0:T(8,128)(2,1)} custom-call(bf16[128,256]{1,0:T(8,128)(2,1)} %qs_ref.1, bf16[128,256]{1,0:T(8,128)(2,1)} %ks_ref.1, bf16[128,256]{1,0:T(8,128)(2,1)} %vs_ref.1, bf16[128,512]{1,0:T(8,128)(2,1)} %ql_ref.1, bf16[128,512]{1,0:T(8,128)(2,1)} %kl_ref.1, bf16[128,512]{1,0:T(8,128)(2,1)} %vl_ref.1, ...), custom_call_target="tpu_custom_call" | custom-call | tf_op jit(solution)/shard_map/layer/pallas_call | solution.py:621
  99.8 1.6 %copy.21 = bf16[32,2048]{1,0:T(8,128)(2,1)} copy(bf16[32,2048]{1,0:T(8,128)(2,1)} %layer.1) | data formatting | bytes 262144

commit v2 on v1

--- a/solution.py
+++ b/solution.py
@@ -220,6 +220,19 @@
     def tp_at(j):
         return (sp, j)
 
+    def flip(index, mask, count):
+        total, bit = 0, 1
+        while bit < count:
+            digit = lax.rem(lax.div(index, bit), 2)
+            total = total + bit * (1 - digit if mask & bit else digit)
+            bit *= 2
+        return total
+
+    z_masks = [*range(0, n_z, 2), *range(1, n_z, 2)]
+    z_order = [flip(chip, m, n_z) for m in z_masks]
+    peers = [flip(tp, m, n_tp) for m in range(n_tp)]
+    out_peers = [*peers[:0:-1], peers[0]]
+
     barrier = pltpu.get_barrier_semaphore()
     for k in range(1, n_sp):
         pl.semaphore_signal(barrier, inc=1, device_id=sp_at(lax.rem(sp + k, n_sp)), device_id_type=pl.DeviceIdType.MESH)
@@ -416,7 +429,7 @@
     for g in range(GROUPS):
         xs[g] = jnp.dot(place[g * cap:(g + 1) * cap, :], normed[...], preferred_element_type=f32).astype(bf16)
     for k in range(n_z):
-        g = lax.rem(chip + k, n_z)
+        g = z_order[k]
         dst = ag.at[core, tp, chip]
         if k == 0:
             pltpu.make_async_copy(xs.at[g], dst, x_recv.at[chip]).start()
@@ -429,46 +442,46 @@
         else:
             mesh_copy(wsend.at[lax.div(j, 2)], wrecv.at[sp], w_send.at[k], w_recv.at[sp], sp_at(j)).start()
 
-    for k in range(n_z):
-        z = lax.rem(chip + k, n_z)
+    for z in z_order:
         piece = ag.at[core, tp, z]
         pltpu.make_async_copy(piece, piece, x_recv.at[z]).wait()
         for m in range(1, n_tp):
-            t = lax.rem(tp + m, n_tp)
-            mesh_copy(piece, piece, g_send.at[m, z], g_recv.at[tp, z], tp_at(t)).start()
+            mesh_copy(piece, piece, g_send.at[m, z], g_recv.at[tp, z], tp_at(peers[m])).start()
         mesh_copy(piece, piece, h_send.at[tp, z], h_recv.at[tp, z], sp_at(sibling)).start()
+    for j in range(n_sp):
+        pltpu.make_async_copy(wrecv.at[j], wrecv.at[j], w_recv.at[j]).wait()
     for load in loads[3:]:
         load.wait()
-    for k in range(n_z):
-        z = lax.rem(chip + k, n_z)
-        for m in range(1, n_tp):
-            t = lax.rem(tp + m, n_tp)
-            piece = ag.at[core, t, z]
-            pltpu.make_async_copy(piece, piece, g_recv.at[t, z]).wait()
-            mesh_copy(piece, piece, h_send.at[t, z], h_recv.at[t, z], sp_at(sibling)).start()
-
-    half_rows = n_z * cap
+
+    other = 1 - core
     lane_c = lax.broadcasted_iota(jnp.int32, (cap, rows), 1)
     sub_c = lax.broadcasted_iota(jnp.int32, (cap, rows), 0)
-    for j in range(n_sp):
-        pltpu.make_async_copy(wrecv.at[j], wrecv.at[j], w_recv.at[j]).wait()
-
-    def slot_weights(c):
-        parts = []
-        for z in range(n_z):
-            row = wrecv[2 * z + c, pl.ds(core, 1), :]
-            parts.append(jnp.sum(jnp.where(sub_c == lane_c, row, 0.0), axis=1, keepdims=True))
-        return jnp.concatenate(parts, axis=0)
-
-    def up_proj(c):
-        step = min(256, ffw)
+    step = min(256, ffw)
+    half = (n_z // 2) * cap
+
+    def slot_weights(c, z):
+        row = wrecv[2 * z + c, pl.ds(core, 1), :]
+        return jnp.sum(jnp.where(sub_c == lane_c, row, 0.0), axis=1, keepdims=True)
+
+    for p in range(2):
+        zs_p = z_order[p * (n_z // 2):(p + 1) * (n_z // 2)]
+        for z in zs_p:
+            for m in range(1, n_tp):
+                piece = ag.at[core, peers[m], z]
+                pltpu.make_async_copy(piece, piece, g_recv.at[peers[m], z]).wait()
+                mesh_copy(piece, piece, h_send.at[peers[m], z], h_recv.at[peers[m], z], sp_at(sibling)).start()
+        for z in zs_p:
+            for t in range(n_tp):
+                piece = ag.at[other, t, z]
+                pltpu.make_async_copy(piece, piece, h_recv.at[t, z]).wait()
+        weights = jnp.concatenate([slot_weights(c, z) for c in (other, core) for z in zs_p], axis=0)
 
         def body(n, carry):
             part = pl.ds(pl.multiple_of(n * step, step), step)
-            gate = jnp.zeros((half_rows, step), f32)
-            upper = jnp.zeros((half_rows, step), f32)
+            gate = jnp.zeros((2 * half, step), f32)
+            upper = jnp.zeros((2 * half, step), f32)
             for t in range(n_tp):
-                x = ag[c, t].reshape(half_rows, cols)
+                x = jnp.concatenate([ag[c, t, z] for c in (other, core) for z in zs_p], axis=0)
                 gate = gate + jnp.dot(x, wg[t * cols:(t + 1) * cols, part], preferred_element_type=f32)
                 upper = upper + jnp.dot(x, wu[t * cols:(t + 1) * cols, part], preferred_element_type=f32)
             hid[:, part] = (gate / (1.0 + jnp.exp(-gate)) * upper).astype(bf16)
@@ -476,49 +489,42 @@
 
         lax.fori_loop(0, ffw // step, body, 0)
 
-    def down_proj(t, weights):
-        part = pl.ds(pl.multiple_of(t * cols, cols), cols)
-        return jnp.dot(hid[...], wd[:, part], preferred_element_type=f32) * weights
-
-    other = 1 - core
-    up_proj(core)
-    own_weights = slot_weights(core)
-    for k in range(1, n_tp + 1):
-        t = lax.rem(tp + k, n_tp)
-        own_y[k - 1] = down_proj(t, own_weights)
-    for t in range(n_tp):
-        for z in range(n_z):
-            piece = ag.at[other, t, z]
-            pltpu.make_async_copy(piece, piece, h_recv.at[t, z]).wait()
-    up_proj(other)
-    other_weights = slot_weights(other)
-    for k in range(1, n_tp + 1):
-        t = lax.rem(tp + k, n_tp)
-        cs[k - 1] = down_proj(t, other_weights).astype(bf16)
-        mesh_copy(cs.at[k - 1], cr.at[k - 1], c_send.at[k - 1], c_recv.at[k - 1], sp_at(sibling)).start()
-    summed = None
-    for k in range(1, n_tp + 1):
-        t = lax.rem(tp + k, n_tp)
-        pltpu.make_async_copy(cr.at[k - 1], cr.at[k - 1], c_recv.at[k - 1]).wait()
-        both = own_y[k - 1] + cr[k - 1].astype(f32)
-        if k < n_tp:
-            ts[k - 1] = both.astype(bf16)
-            mesh_copy(ts.at[k - 1], rr.at[tp], t_send.at[k], t_recv.at[tp], tp_at(t)).start()
+        def join(k):
+            pltpu.make_async_copy(cr.at[p, k], cr.at[p, k], c_recv.at[p, k]).wait()
+            both = own_y[p, k] + cr[p, k].astype(f32)
+            if k == n_tp - 1:
+                own_y[p, k] = both
+                return
+            for i in range(n_z // 2):
+                kz = p * (n_z // 2) + i
+                ts[k, kz] = both[i * cap:(i + 1) * cap].astype(bf16)
+                mesh_copy(
+                    ts.at[k, kz], rr.at[tp, kz], t_send.at[k, kz], t_recv.at[tp, kz], tp_at(out_peers[k])
+                ).start()
+
+        for k in range(n_tp):
+            part = pl.ds(pl.multiple_of(out_peers[k] * cols, cols), cols)
+            y = jnp.dot(hid[...], wd[:, part], preferred_element_type=f32) * weights
+            cs[p, k] = y[:half].astype(bf16)
+            mesh_copy(cs.at[p, k], cr.at[p, k], c_send.at[p, k], c_recv.at[p, k], sp_at(sibling)).start()
+            own_y[p, k] = y[half:]
+            if k:
+                join(k - 1)
+        join(n_tp - 1)
+
+    for kz in range(n_z):
+        z = z_order[kz]
+        i = kz % (n_z // 2)
+        total = own_y[kz // (n_z // 2), n_tp - 1, i * cap:(i + 1) * cap, :]
+        for m in range(1, n_tp):
+            src = peers[m]
+            pltpu.make_async_copy(rr.at[src, kz], rr.at[src, kz], t_recv.at[src, kz]).wait()
+            total = total + rr[src, kz].astype(f32)
+        zs[kz] = total.astype(bf16)
+        if kz:
+            mesh_copy(zs.at[kz], zr.at[chip], z_send.at[kz], z_recv.at[chip], sp_at(2 * z + core)).start()
         else:
-            own_y[k - 1] = both
-    for k in range(1, n_tp):
-        tp_wait_recv(rr, t_recv, lax.rem(tp + k, n_tp))
-    for k in range(1, n_z + 1):
-        z = lax.rem(chip + k, n_z)
-        part = pl.ds(pl.multiple_of(z * cap, cap), cap)
-        total = own_y[n_tp - 1, part, :]
-        for m in range(1, n_tp):
-            total = total + rr[lax.rem(tp + m, n_tp), part, :].astype(f32)
-        zs[k - 1] = total.astype(bf16)
-        if k < n_z:
-            mesh_copy(zs.at[k - 1], zr.at[chip], z_send.at[k], z_recv.at[chip], sp_at(2 * z + core)).start()
-        else:
-            pltpu.make_async_copy(zs.at[k - 1], zr.at[chip], z_recv.at[chip]).start()
+            pltpu.make_async_copy(zs.at[kz], zr.at[chip], z_recv.at[chip]).start()
     for z in range(n_z):
         pltpu.make_async_copy(zr.at[z], zr.at[z], z_recv.at[z]).wait()
     expert_mix = lax.dot_general(
@@ -555,17 +561,20 @@
         t = lax.rem(tp + k, n_tp)
         mesh_copy(pb.at[k - 1], rp.at[tp], p_send.at[k], p_recv.at[tp], tp_at(t)).wait_send()
         mesh_copy(st, rst.at[tp], s_send.at[k], s_recv.at[tp], tp_at(t)).wait_send()
-        mesh_copy(ts.at[k - 1], rr.at[tp], t_send.at[k], t_recv.at[tp], tp_at(t)).wait_send()
         mesh_copy(fs.at[t], fr.at[tp], f_send.at[k], f_recv.at[tp], tp_at(t)).wait_send()
         for z in range(n_z):
             piece = ag.at[core, tp, z]
-            mesh_copy(piece, piece, g_send.at[k, z], g_recv.at[tp, z], tp_at(t)).wait_send()
+            mesh_copy(piece, piece, g_send.at[k, z], g_recv.at[tp, z], tp_at(peers[k])).wait_send()
+            mesh_copy(
+                ts.at[k - 1, z], rr.at[tp, z], t_send.at[k - 1, z], t_recv.at[tp, z], tp_at(out_peers[k - 1])
+            ).wait_send()
     for k in range(1, n_z):
-        g = lax.rem(chip + k, n_z)
+        g = z_order[k]
         mesh_copy(xs.at[g], ag.at[core, tp, chip], x_send.at[k], x_recv.at[chip], sp_at(2 * g + core)).wait_send()
-        mesh_copy(zs.at[k - 1], zr.at[chip], z_send.at[k], z_recv.at[chip], sp_at(2 * g + core)).wait_send()
+        mesh_copy(zs.at[k], zr.at[chip], z_send.at[k], z_recv.at[chip], sp_at(2 * g + core)).wait_send()
     for t in range(n_tp):
-        mesh_copy(cs.at[t], cr.at[t], c_send.at[t], c_recv.at[t], sp_at(sibling)).wait_send()
+        for p in range(2):
+            mesh_copy(cs.at[p, t], cr.at[p, t], c_send.at[p, t], c_recv.at[p, t], sp_at(sibling)).wait_send()
         for z in range(n_z):
             piece = ag.at[core, t, z]
             mesh_copy(piece, piece, h_send.at[t, z], h_recv.at[t, z], sp_at(sibling)).wait_send()
@@ -605,16 +614,16 @@
         V((GROUPS, 8, rows), f32), V((n_sp, 8, rows), f32),
         V((2, n_tp, n_z, cap, cols), bf16),
         V((width, ffw), bf16), V((width, ffw), bf16), V((ffw, width), bf16),
-        V((half, ffw), bf16), V((n_tp, half, cols), f32),
-        V((n_tp, half, cols), bf16), V((n_tp, half, cols), bf16),
-        V((n_tp, half, cols), bf16), V((n_tp, half, cols), bf16),
+        V((half, ffw), bf16), V((2, n_tp, half // 2, cols), f32),
+        V((2, n_tp, half // 2, cols), bf16), V((2, n_tp, half // 2, cols), bf16),
+        V((n_tp - 1, n_z, cap, cols), bf16), V((n_tp, n_z, cap, cols), bf16),
         V((n_z, cap, cols), bf16), V((n_z, cap, cols), bf16),
         V((n_tp, rows // n_tp, cols), f32), V((n_tp, rows // n_tp, cols), f32),
         dma((6,)), dma((4, n_sp)), dma((4, n_sp)), dma((n_sp,)), dma((n_sp,)),
         dma((n_tp,)), dma((n_tp,)), dma((n_tp,)), dma((n_tp,)),
         dma((n_z,)), dma((n_z,)), dma((n_sp,)), dma((n_sp,)),
         dma((n_tp, n_z)), dma((n_tp, n_z)), dma((n_tp, n_z)), dma((n_tp, n_z)),
-        dma((n_tp,)), dma((n_tp,)), dma((n_tp,)), dma((n_tp,)),
+        dma((2, n_tp)), dma((2, n_tp)), dma((n_tp, n_z)), dma((n_tp, n_z)),
         dma((n_z,)), dma((n_z,)), dma((n_tp,)), dma((n_tp,)),
     ]
     dims = (n_sp, n_tp, rows, cols, cap, small_heads, hs, hl)

time: 102 us -> 94.9 us (0.930)
  Pallas kernels: 98.5 us -> 91.8 us
    pallas_call x1, Pallas kernels: 98.5 us -> 91.8 us  [fast_local(): pl.pallas_call(functools.partial(fast_kernel, dims), out_shape=jax.ShapeD...]
where the time goes in v2:
time: 94.9 us; the launch traced here: 94.7 us
  Pallas kernels  91.8 us (97%)
  local copies, waits for them, and re-layouts  2.19 us (2%)
    pallas_call x1, Pallas kernels, fast_local(): pl.pallas_call(functools.partial(fast_kernel, dims), out_shape=jax.ShapeD...  91.8 us

profile of v2, /device:TPU:0, one launch (start us, length us, event | category | flops | bytes accessed | tf_op | source)
XLA Modules:
  0.0 94.7 jit_solution(12000392304474181073)
XLA Ops:
  0.0 0.7 broadcast_in_dim.30
  0.7 0.6 broadcast_in_dim.24.bias_ref
  1.3 91.8 %layer.1 = bf16[32,2048]{1,0:T(8,128)(2,1)} custom-call(bf16[128,256]{1,0:T(8,128)(2,1)} %qs_ref.1, bf16[128,256]{1,0:T(8,128)(2,1)} %ks_ref.1, bf16[128,256]{1,0:T(8,128)(2,1)} %vs_ref.1, bf16[128,512]{1,0:T(8,128)(2,1)} %ql_ref.1, bf16[128,512]{1,0:T(8,128)(2,1)} %kl_ref.1, bf16[128,512]{1,0:T(8,128)(2,1)} %vl_ref.1, ...), custom_call_target="tpu_custom_call" | custom-call | tf_op jit(solution)/shard_map/layer/pallas_call | solution.py:630
  93.2 1.6 %copy.21 = bf16[32,2048]{1,0:T(8,128)(2,1)} copy(bf16[32,2048]{1,0:T(8,128)(2,1)} %layer.1) | data formatting | bytes 262144

commit v3 on v2

--- a/solution.py
+++ b/solution.py
@@ -228,7 +228,7 @@
             bit *= 2
         return total
 
-    z_masks = [*range(0, n_z, 2), *range(1, n_z, 2)]
+    z_masks = [0, n_z - 1, *range(1, n_z - 1)]
     z_order = [flip(chip, m, n_z) for m in z_masks]
     peers = [flip(tp, m, n_tp) for m in range(n_tp)]
     out_peers = [*peers[:0:-1], peers[0]]
@@ -254,25 +254,35 @@
     for h in range(small_heads):
         part = slice(h * hs, (h + 1) * hs)
         pack_a[h] = jnp.concatenate([qs_ref[:, part], ks_ref[:, part]], axis=1)
-        pack_v[h] = jnp.concatenate([vs_ref[:, part], jnp.zeros((rows, hl - hs), bf16)], axis=1)
+        pack_v[h] = jnp.concatenate([vs_ref[:rows // 2, part], vs_ref[rows // 2:, part]], axis=1)
 
     pl.semaphore_wait(barrier, n_sp + n_tp - 2)
+
+    half_block = pl.ds(0, rows // 2)
 
     def head_copies(j, slot):
         if j < small_heads:
-            pairs = [(0, pack_a.at[j], rq), (2, pack_v.at[j], rv)]
+            pairs = [(0, pack_a.at[j], rq.at[slot]), (2, pack_v.at[j], rv.at[slot, half_block])]
         else:
             part = pl.ds((j - small_heads) * hl, hl)
-            pairs = [(0, ql_ref.at[:, part], rq), (1, kl_ref.at[:, part], rk), (2, vl_ref.at[:, part], rv)]
-        pairs.append((3, bias_ref.at[j], rb))
-        return [(kind, src, dst.at[slot]) for kind, src, dst in pairs]
+            pairs = [
+                (0, ql_ref.at[:, part], rq.at[slot]),
+                (1, kl_ref.at[:, part], rk.at[slot]),
+                (2, vl_ref.at[:, part], rv.at[slot]),
+            ]
+        pairs.append((3, bias_ref.at[j], rb.at[slot]))
+        return pairs
+
+    for distance in range(n_z):
+        for j in range(n_sp):
+            hops = jnp.maximum(j // 2 - chip, chip - j // 2)
+
+            @pl.when((hops == distance) & (j != sp))
+            def _():
+                for kind, src, dst in head_copies(j, sp):
+                    mesh_copy(src, dst, q_send.at[kind, j], q_recv.at[kind, sp], sp_at(j)).start()
 
     for j in range(n_sp):
-        @pl.when(j != sp)
-        def _():
-            for kind, src, dst in head_copies(j, sp):
-                mesh_copy(src, dst, q_send.at[kind, j], q_recv.at[kind, sp], sp_at(j)).start()
-
         @pl.when(j == sp)
         def _():
             for kind, src, dst in head_copies(j, j):
@@ -303,14 +313,19 @@
         )
 
     for j in range(n_sp):
-        for kind in (0, 2, 3):
-            dst = (rq, None, rv, rb)[kind].at[j]
+        for kind in (0, 3):
+            dst = (rq, None, None, rb)[kind].at[j]
             pltpu.make_async_copy(dst, dst, q_recv.at[kind, j]).wait()
+
+    def unfold(packed):
+        tall = jnp.concatenate([packed[:, :hs], packed[:, hs:]], axis=0)
+        return jnp.concatenate([tall, jnp.zeros_like(tall)], axis=1)
 
     @pl.when(jnp.logical_not(is_small))
     def _():
         for j in range(n_sp):
             pltpu.make_async_copy(rk.at[j], rk.at[j], q_recv.at[1, j]).wait()
+            pltpu.make_async_copy(rv.at[j], rv.at[j], q_recv.at[2, j]).wait()
             aq[pl.ds(j * rows, rows), :] = rq[j]
             ak[pl.ds(j * rows, rows), :] = rk[j]
 
@@ -318,6 +333,9 @@
     def _():
         lane = lax.broadcasted_iota(jnp.int32, (rows, hl), 1)
         for j in range(n_sp):
+            folded = rv.at[j, half_block]
+            pltpu.make_async_copy(folded, folded, q_recv.at[2, j]).wait()
+            rv[j] = unfold(folded[...])
             both = rq[j]
             aq[pl.ds(j * rows, rows), :] = jnp.where(lane < hs, both, jnp.zeros_like(both))
             ak[pl.ds(j * rows, rows), :] = jnp.concatenate([both[:, hs:], both[:, :hs]], axis=1)
@@ -353,6 +371,10 @@
         total = total + jnp.dot(stick.astype(bf16), values, preferred_element_type=f32)
         return total, later + run[:, 0:1]
 
+    def head_back(d, small):
+        src, dst = (ao.at[d, half_block], ra.at[sp, half_block]) if small else (ao.at[d], ra.at[sp])
+        return mesh_copy(src, dst, a_send.at[d], a_recv.at[sp], sp_at(d))
+
     for qi in range(n_sp // 2):
         query = aq[qi * span:(qi + 1) * span, :]
         carry = tile(query, qi, True, jnp.zeros((span, hl), f32), jnp.zeros((span, 1), f32))
@@ -362,30 +384,44 @@
             carry = lax.fori_loop(0, qi, visit, carry)
         for half in range(2):
             d = 2 * qi + half
-            ao[d] = carry[0][half * rows:(half + 1) * rows].astype(bf16)
+            block = carry[0][half * rows:(half + 1) * rows].astype(bf16)
+
+            @pl.when(is_small)
+            def _():
+                ao[d, :rows // 2, :] = jnp.concatenate([block[:rows // 2, :hs], block[rows // 2:, :hs]], axis=1)
+
+            @pl.when(jnp.logical_not(is_small))
+            def _():
+                ao[d] = block
         for half in range(2):
             d = 2 * qi + half
-
-            @pl.when(d != sp)
-            def _():
-                mesh_copy(ao.at[d], ra.at[sp], a_send.at[d], a_recv.at[sp], sp_at(d)).start()
+            for small in (True, False):
+                @pl.when((d != sp) & (is_small if small else jnp.logical_not(is_small)))
+                def _():
+                    head_back(d, small).start()
+
+            if d < small_heads:
+                own = pltpu.make_async_copy(ao.at[d, half_block], ra.at[d, half_block], a_recv.at[d])
+            else:
+                own = pltpu.make_async_copy(ao.at[d], ra.at[d], a_recv.at[d])
 
             @pl.when(d == sp)
             def _():
-                pltpu.make_async_copy(ao.at[d], ra.at[d], a_recv.at[d]).start()
+                own.start()
 
     for load in loads[:3]:
         load.wait()
     for j in range(n_sp):
-        pltpu.make_async_copy(ra.at[j], ra.at[j], a_recv.at[j]).wait()
-    att_small = jnp.concatenate([ra[j][:, :hs] for j in range(small_heads)], axis=1)
+        landed = ra.at[j, half_block] if j < small_heads else ra.at[j]
+        pltpu.make_async_copy(landed, landed, a_recv.at[j]).wait()
+    att_small = jnp.concatenate([unfold(ra[j, :rows // 2, :])[:, :hs] for j in range(small_heads)], axis=1)
     att_large = jnp.concatenate([ra[j] for j in range(small_heads, n_sp)], axis=1)
 
     def tp_wait_recv(buf, sem, src):
         pltpu.make_async_copy(buf.at[src], buf.at[src], sem.at[src]).wait()
 
     for k in range(1, n_tp + 1):
-        t = lax.rem(tp + k, n_tp)
+        t = out_peers[k - 1]
         part = pl.ds(pl.multiple_of(t * cols, cols), cols)
         term = jnp.dot(att_small, wos[:, part], preferred_element_type=f32)
         term = term + jnp.dot(att_large, wol[:, part], preferred_element_type=f32)
@@ -551,15 +587,16 @@
         out_ref[:, part] = (blocks[t] * inverse * g2_ref[:, part] + b2_ref[:, part]).astype(bf16)
 
     for d in range(n_sp):
-        @pl.when(d != sp)
-        def _():
-            mesh_copy(ao.at[d], ra.at[sp], a_send.at[d], a_recv.at[sp], sp_at(d)).wait_send()
+        for small in (True, False):
+            @pl.when((d != sp) & (is_small if small else jnp.logical_not(is_small)))
+            def _():
+                head_back(d, small).wait_send()
     for k in range(1, n_sp):
         j = lax.rem(sp + k, n_sp)
         mesh_copy(wsend.at[lax.div(j, 2)], wrecv.at[sp], w_send.at[k], w_recv.at[sp], sp_at(j)).wait_send()
     for k in range(1, n_tp):
         t = lax.rem(tp + k, n_tp)
-        mesh_copy(pb.at[k - 1], rp.at[tp], p_send.at[k], p_recv.at[tp], tp_at(t)).wait_send()
+        mesh_copy(pb.at[k - 1], rp.at[tp], p_send.at[k], p_recv.at[tp], tp_at(out_peers[k - 1])).wait_send()
         mesh_copy(st, rst.at[tp], s_send.at[k], s_recv.at[tp], tp_at(t)).wait_send()
         mesh_copy(fs.at[t], fr.at[tp], f_send.at[k], f_recv.at[tp], tp_at(t)).wait_send()
         for z in range(n_z):
@@ -602,7 +639,7 @@
     V = pltpu.VMEM
     half = n_z * cap
     scratch = [
-        V((small_heads, rows, hl), bf16), V((small_heads, rows, hl), bf16),
+        V((small_heads, rows, hl), bf16), V((small_heads, rows // 2, hl), bf16),
         V((n_sp, rows, hl), bf16), V((n_sp, rows, hl), bf16), V((n_sp, rows, hl), bf16),
         V((n_sp, 8, rows), f32),
         V((n_sp * rows, hl), bf16), V((n_sp * rows, hl), bf16),

time: 94.9 us -> 92.9 us (0.979)
  Pallas kernels: 91.8 us -> 89.8 us
    pallas_call x1, Pallas kernels: 91.8 us -> 89.8 us  [fast_local(): pl.pallas_call(functools.partial(fast_kernel, dims), out_shape=jax.ShapeD...]
where the time goes in v3:
time: 92.9 us; the launch traced here: 92.7 us
  Pallas kernels  89.8 us (97%)
  local copies, waits for them, and re-layouts  2.19 us (2%)
    pallas_call x1, Pallas kernels, fast_local(): pl.pallas_call(functools.partial(fast_kernel, dims), out_shape=jax.ShapeD...  89.8 us

profile of v3, /device:TPU:0, one launch (start us, length us, event | category | flops | bytes accessed | tf_op | source)
XLA Modules:
  0.0 92.7 jit_solution(8507706162599944273)
XLA Ops:
  0.0 0.7 broadcast_in_dim.30
  0.7 0.6 broadcast_in_dim.24.bias_ref
  1.3 89.8 %layer.1 = bf16[32,2048]{1,0:T(8,128)(2,1)} custom-call(bf16[128,256]{1,0:T(8,128)(2,1)} %qs_ref.1, bf16[128,256]{1,0:T(8,128)(2,1)} %ks_ref.1, bf16[128,256]{1,0:T(8,128)(2,1)} %vs_ref.1, bf16[128,512]{1,0:T(8,128)(2,1)} %ql_ref.1, bf16[128,512]{1,0:T(8,128)(2,1)} %kl_ref.1, bf16[128,512]{1,0:T(8,128)(2,1)} %vl_ref.1, ...), custom_call_target="tpu_custom_call" | custom-call | tf_op jit(solution)/shard_map/layer/pallas_call | solution.py:667
  91.2 1.6 %copy.21 = bf16[32,2048]{1,0:T(8,128)(2,1)} copy(bf16[32,2048]{1,0:T(8,128)(2,1)} %layer.1) | data formatting | bytes 262144
